TPU v7x, 32 devices: a whole 2x2x4 slice. The times are simulated.
32 devices in a mesh: sp: 8 (over z, core), tp: 4 (over y, x).
Axes of the slice: x: 2, y: 2, z: 4, core: 2. Of those that a mesh axis runs over, the one named last changes fastest.
Arguments:
- queries: bfloat16 [2048, 1024], P('sp', 'tp'), may hold values from -250 to 250
- keys_values: bfloat16 [2, 2048, 256], P(None, 'sp'), may hold values from -8 to 8
- sink_logits: float32 [16], P('tp'), may hold values from 1 to 5
- proj_weight: bfloat16 [1024, 2048], P('tp'), may hold values from -0.75 to 0.75
- residual: bfloat16 [2048, 2048], P('sp', 'tp'), may hold values from -6 to 6
- norm_gain: float32 [2048], replicated, may hold values from 0.1 to 1.9
- routes: int32 [2048, 2], P('sp'), may hold values from 0 to 7, all different within a row; in each aligned block of 256 rows (0 to 255, 256 to 511, ...) at most 128 rows name the same one
- route_weights: float32 [2048, 2], P('sp'), may hold values from 0.2 to 1
- gate_weight: bfloat16 [8, 2048, 2048], P('sp', None, 'tp'), may hold values from -0.125 to 0.125
- up_weight: bfloat16 [8, 2048, 2048], P('sp', None, 'tp'), may hold values from -0.125 to 0.125
- down_weight: bfloat16 [8, 2048, 2048], P('sp', None, 'tp'), may hold values from -0.125 to 0.125
- shared_gate: bfloat16 [2048, 2048], P(None, 'tp'), may hold values from -0.125 to 0.125
- shared_up: bfloat16 [2048, 2048], P(None, 'tp'), may hold values from -0.125 to 0.125
- shared_down: bfloat16 [2048, 2048], P(None, 'tp'), may hold values from -0.125 to 0.125
Outputs:
- output: bfloat16 [2048, 2048], P('sp', 'tp')
Inputs may be any that keep to these rules, and one draw needn't show every extreme that they name: `routes`: the 2 experts of a position differ. In each aligned block of 256 positions no expert is named by more than 128 positions, and in some block one expert is named by exactly 128.
All inputs are finite; a program needn't handle non-finite values.
Results may differ from a plain program's by a relative error of at most 0.0067.
Values may be sent and summed in bfloat16 or wider, within the bound.
A program may use at most 64 MiB of HBM per device.

v0:
```python
import jax
import jax.numpy as jnp
from jax import lax
from jax.sharding import PartitionSpec as P

D = 2048
HEADS = 16
KV_HEADS = 4
HEAD_WIDTH = 64
WINDOW = 128
TOP_K = 2
EXP_DEV = 1
TOK_DEV = 256
norm_eps = 1e-06


def passed_along(value, axis, steps):
    count = lax.axis_size(axis)
    initial, last = (max(0, -steps), min(count, count - steps))
    return lax.ppermute(value, axis, [(source, source + steps) for source in range(initial, last)])


def per_device(
    queries,
    keys_values,
    sink_logits,
    proj_weight,
    residual,
    norm_gain,
    routes,
    route_weights,
    gate_weight,
    up_weight,
    down_weight,
    shared_gate,
    shared_up,
    shared_down,
):
    tp_index = lax.axis_index("tp")
    sp_index = lax.axis_index("sp")
    sp_count = lax.axis_size("sp")
    tp_count = lax.axis_size("tp")
    heads_here = sink_logits.shape[0]
    col_width = residual.shape[1]
    blocks = TOK_DEV // WINDOW
    kv_group = HEADS // KV_HEADS
    earlier_keys = passed_along(keys_values[:, TOK_DEV - WINDOW :, :], "sp", 1)
    extended = jnp.concatenate([earlier_keys, keys_values], axis=1)
    extended = extended.reshape(2, TOK_DEV + WINDOW, KV_HEADS, HEAD_WIDTH)
    head_ids = tp_index * heads_here + jnp.arange(heads_here, dtype=jnp.int32)
    chosen = jnp.take(extended, head_ids // kv_group, axis=2)
    earlier = chosen[:, :TOK_DEV].reshape(2, blocks, WINDOW, heads_here, HEAD_WIDTH)
    later = chosen[:, WINDOW:].reshape(2, blocks, WINDOW, heads_here, HEAD_WIDTH)
    banded = jnp.concatenate([earlier, later], axis=2)
    query_blocks = queries.reshape(blocks, WINDOW, heads_here, HEAD_WIDTH)
    score_matrix = jnp.einsum(
        "bqhd,bkhd->bhqk", query_blocks, banded[0], preferred_element_type=jnp.float32
    ) * HEAD_WIDTH ** (-0.5)
    query_pos = jnp.arange(WINDOW, dtype=jnp.int32)[:, None]
    key_pos = jnp.arange(2 * WINDOW, dtype=jnp.int32)[None, :]
    distance = WINDOW + query_pos - key_pos
    absolute = (
        sp_index * TOK_DEV
        + jnp.arange(blocks, dtype=jnp.int32)[:, None, None] * WINDOW
        - WINDOW
        + key_pos[None]
    )
    allowed = (distance >= 0)[None] & (distance < WINDOW)[None] & (absolute >= 0)
    masked = jnp.where(allowed[:, None], score_matrix, -jnp.inf)
    sink_value = sink_logits[None, :, None, None]
    highest = jnp.maximum(jnp.max(masked, axis=-1, keepdims=True), sink_value)
    weights_exp = jnp.exp(masked - highest)
    denominator = jnp.sum(weights_exp, axis=-1, keepdims=True) + jnp.exp(sink_value - highest)
    softmax_weights = (weights_exp / denominator).astype(jnp.bfloat16)
    attended_values = jnp.einsum(
        "bhqk,bkhd->bqhd", softmax_weights, banded[1], preferred_element_type=jnp.float32
    )
    attended_values = attended_values.astype(jnp.bfloat16).reshape(TOK_DEV, heads_here * HEAD_WIDTH)
    attended_all = lax.all_gather(attended_values, "tp", axis=1, tiled=True)
    weight_rows = proj_weight.shape[0]
    column_share = lax.all_to_all(
        proj_weight.reshape(weight_rows, tp_count, col_width),
        "tp",
        split_axis=1,
        concat_axis=0,
        tiled=True,
    )
    column_share = column_share.reshape(HEADS * HEAD_WIDTH, col_width)
    feature_sum = jnp.dot(attended_all, column_share, preferred_element_type=jnp.float32)
    stream_cols = (feature_sum + residual.astype(jnp.float32)).astype(jnp.bfloat16)
    stream_rows = lax.all_gather(stream_cols, "tp", axis=1, tiled=True)
    gate_eff = (norm_gain[None, :, None] * gate_weight.astype(jnp.float32)).astype(jnp.bfloat16)
    up_eff = (norm_gain[None, :, None] * up_weight.astype(jnp.float32)).astype(jnp.bfloat16)
    shared_gate_eff = (norm_gain[:, None] * shared_gate.astype(jnp.float32)).astype(jnp.bfloat16)
    shared_up_eff = (norm_gain[:, None] * shared_up.astype(jnp.float32)).astype(jnp.bfloat16)
    experts_total = EXP_DEV * sp_count
    capacity = 2 * TOK_DEV * TOP_K // experts_total
    rows_per_expert = sp_count * capacity
    flat_routes = routes.reshape(-1)
    onehot = (flat_routes[:, None] == jnp.arange(experts_total, dtype=jnp.int32)[None, :]).astype(
        jnp.int32
    )
    before = jnp.cumsum(onehot, axis=0) - onehot
    slot_rank = jnp.sum(before * onehot, axis=1)
    slot_index = (
        flat_routes % EXP_DEV * rows_per_expert + flat_routes // EXP_DEV * capacity + slot_rank
    )
    token_of = jnp.arange(TOK_DEV * TOP_K, dtype=jnp.int32) // TOP_K
    slot_owner = (
        jnp.full((EXP_DEV * rows_per_expert,), TOK_DEV, jnp.int32).at[slot_index].set(token_of)
    )
    picked_rows = jnp.take(stream_rows, slot_owner, axis=0, mode="fill", fill_value=0)
    arrived = lax.all_to_all(
        picked_rows.reshape(EXP_DEV, sp_count, capacity, stream_rows.shape[1]),
        "sp",
        split_axis=1,
        concat_axis=1,
        tiled=True,
    )
    arrived = arrived.reshape(EXP_DEV, rows_per_expert, D)
    routed_squares = jnp.sum(jnp.square(arrived.astype(jnp.float32)), axis=-1)
    gate_sum = jnp.einsum("erd,edf->erf", arrived, gate_eff, preferred_element_type=jnp.float32)
    up_sum = jnp.einsum("erd,edf->erf", arrived, up_eff, preferred_element_type=jnp.float32)
    own_squares = jnp.sum(jnp.square(stream_rows.astype(jnp.float32)), axis=-1)
    shared_gate_sum = jnp.dot(stream_rows, shared_gate_eff, preferred_element_type=jnp.float32)
    shared_up_sum = jnp.dot(stream_rows, shared_up_eff, preferred_element_type=jnp.float32)
    routed_scale = lax.rsqrt(routed_squares / D + norm_eps)[..., None]
    own_scale = lax.rsqrt(own_squares / D + norm_eps)[:, None]
    hidden = (jax.nn.silu(routed_scale * gate_sum) * (routed_scale * up_sum)).astype(jnp.bfloat16)
    shared_hidden = (jax.nn.silu(own_scale * shared_gate_sum) * (own_scale * shared_up_sum)).astype(
        jnp.bfloat16
    )
    routed_piece = lax.all_gather(hidden, "tp", axis=2, tiled=True)
    own_piece = lax.all_gather(shared_hidden[None], "tp", axis=2, tiled=True)
    expert_out = jnp.einsum(
        "erf,efd->erd", routed_piece, down_weight, preferred_element_type=jnp.float32
    )
    shared_out = jnp.dot(own_piece[0], shared_down, preferred_element_type=jnp.float32)
    outgoing = expert_out.astype(jnp.bfloat16).reshape(EXP_DEV, sp_count, capacity, col_width)
    returned = lax.all_to_all(outgoing, "sp", split_axis=1, concat_axis=1, tiled=True).reshape(
        EXP_DEV * rows_per_expert, col_width
    )
    picked = jnp.take(returned, slot_index, axis=0).reshape(TOK_DEV, TOP_K, col_width)
    routed_sum = jnp.einsum("nk,nkd->nd", route_weights, picked.astype(jnp.float32))
    return (stream_cols.astype(jnp.float32) + shared_out + routed_sum).astype(jnp.bfloat16)


def solution(mesh):
    placed = (
        P("sp", "tp"),
        P(None, "sp", None),
        P("tp"),
        P("tp", None),
        P("sp", "tp"),
        P(),
        P("sp", None),
        P("sp", None),
        P("sp", None, "tp"),
        P("sp", None, "tp"),
        P("sp", None, "tp"),
        P(None, "tp"),
        P(None, "tp"),
        P(None, "tp"),
    )
    return jax.shard_map(
        per_device, mesh=mesh, in_specs=placed, out_specs=P("sp", "tp"), check_vma=False
    )
```

profile of v0, /device:TPU:0, one launch (start us, length us, event | category | flops | bytes accessed | tf_op | source)
XLA Modules:
  0.0 293.3 jit_solution(9455327325811044780)
XLA Ops:
  6.5 1.2 copy.63
  7.8 3.2 %collective-permute-start = (bf16[2,128,256]{1,2,0:T(8,128)(2,1)S(1)}, bf16[2,128,256]{1,2,0:T(8,128)(2,1)}, u32[]{:S(2)}, u32[]{:S(2)}) collective-permute-start(bf16[2,128,256]{1,2,0:T(8,128)(2,1)S(1)} %slice.34), channel_id=1, source_target_pairs={{0,4},{4,8},{8,12},{12,16},{16,20},{20,24},{24,28},{1,5},{5,9},{9,... | collective-permute-start | bytes 393224 | tf_op jit(solution)/shard_map/ppermute | solution.py:20
  11.0 2.3 copy.73
  13.3 4.5 %all-to-all-start = ((bf16[256,4,512]{0,2,1:T(8,128)(2,1)}), bf16[256,4,512]{0,2,1:T(8,128)(2,1)S(1)}, u32[]{:S(2)}, u32[]{:S(2)}) async-start(bf16[256,4,512]{0,2,1:T(8,128)(2,1)} %bitcast.91), calls=%async_computation | async-start | bytes 2097152 | tf_op jit(solution)/shard_map/all_to_all | solution.py:81
  18.7 0.9 reshape.384
  19.6 1.0 pad_maximum_fusion
  20.7 1.4 gather_fusion
  22.0 1.1 select_bitcast_fusion
  24.0 1.0 reshape.382
  25.8 1.0 reshape.383
  27.6 1.5 fusion.48
  30.0 12.7 %all_gather.12 = bf16[256,1024]{0,1:T(8,128)(2,1)} all-gather(bf16[256,256]{0,1:T(8,128)(2,1)S(1)} %bitcast.95), channel_id=1, replica_groups=mesh['sp'=8,'tp'=4] {'tp'}, dimensions={1}, use_global_device_ids=true | all-gather | bytes 655360 | tf_op jit(solution)/shard_map/all_gather | solution.py:79
  42.7 1.3 copy.74
  44.0 2.6 fusion.25
  47.1 1.1 reduce-window.6
  48.9 2.4 scatter_custom_fusion
  51.4 20.4 %all-gather.6.cloned.1.call-done = bf16[256,2048]{1,0:T(8,128)(2,1)} async-done(((bf16[256,512]{1,0:T(8,128)(2,1)}), bf16[256,2048]{1,0:T(8,128)(2,1)}) %all-gather.6.cloned.1.call-update) | async-done | bytes 1048592 | tf_op jit(solution)/shard_map/all_gather | solution.py:91
  71.8 10.2 %gather_fusion.1 = bf16[1024,2048]{1,0:T(8,128)(2,1)} fusion(bf16[256,2048]{1,0:T(8,128)(2,1)} %all-gather.6.cloned.1.call-done, s32[1024]{0:T(1024)S(1)} %fusion.39), kind=kCustom, calls=%fused_computation.1 | custom fusion | bytes 8392704 | tf_op jit(solution)/shard_map/jit(_take)/gather | solution.py:112
  82.0 2.5 broadcast_select_fusion
  84.5 98.4 %all_to_all.25 = bf16[1,8,128,2048]{3,2,0,1:T(8,128)(2,1)S(1)} all-to-all(bf16[1,8,128,2048]{3,2,0,1:T(8,128)(2,1)S(1)} %broadcast_select_fusion), channel_id=1, replica_groups=mesh['sp'=8,'tp'=4] {'sp'}, dimensions={1} | all-to-all | bytes 8388608 | tf_op jit(solution)/shard_map/all_to_all | solution.py:113
  182.9 0.9 multiply_reduce_fusion
  184.5 2.4 fusion.3
  186.9 3.7 %multiply_convert_fusion.6 = bf16[1024,512]{1,0:T(8,128)(2,1)} fusion(f32[1024,512]{1,0:T(8,128)S(1)} %fusion.3, bf16[1024,2048]{1,0:T(8,128)(2,1)S(1)} %bitcast.89, bf16[1,2048,512]{2,1,0:T(8,128)(2,1)S(1)} %copy-done.11, f32[2048]{0:T(1024)S(1)} %copy-done.14, f32[1024]{0:T(1024)S(1)} %rsqrt_bitcast_fusion), kind=kOutput, calls=%fused_computation.18 | convolution fusion | flops 2154823680 | bytes 9449472 | tf_op jit(solution)/shard_map/erd,edf->erf/dot_general | solution.py:123
  191.0 50.3 %all-gather.10.cloned.1.call-done = bf16[1024,2048]{1,0:T(8,128)(2,1)} async-done(((bf16[1024,512]{1,0:T(8,128)(2,1)}), bf16[1024,2048]{1,0:T(8,128)(2,1)}) %all-gather.10.cloned.1.call-update) | async-done | bytes 4194320 | tf_op jit(solution)/shard_map/all_gather | solution.py:133
  241.3 5.5 %fusion.16 = bf16[1024,512]{1,0:T(8,128)(2,1)} fusion(bf16[1024,2048]{1,0:T(8,128)(2,1)} %all-gather.10.cloned.1.call-done, bf16[1,2048,512]{2,1,0:T(8,128)(2,1)S(1)} %copy-done), kind=kOutput, calls=%fused_computation.24 | convolution fusion | flops 2148007936 | bytes 7340032 | tf_op jit(solution)/shard_map/erf,efd->erd/dot_general | solution.py:135
  246.8 4.6 %all-to-all-start.2 = ((bf16[1,8,128,512]{3,2,0,1:T(8,128)(2,1)}), bf16[1,8,128,512]{3,2,0,1:T(8,128)(2,1)}, u32[]{:S(2)}, u32[]{:S(2)}) async-start(bf16[1,8,128,512]{3,2,0,1:T(8,128)(2,1)} %bitcast.93), calls=%async_computation.2 | async-start | bytes 2097152 | tf_op jit(solution)/shard_map/all_to_all | solution.py:140
  251.4 2.6 fusion.23
  254.0 1.6 fusion.27
  256.3 21.8 %all-to-all-done.2 = bf16[1,8,128,512]{3,2,0,1:T(8,128)(2,1)} async-done(((bf16[1,8,128,512]{3,2,0,1:T(8,128)(2,1)}), bf16[1,8,128,512]{3,2,0,1:T(8,128)(2,1)}, u32[]{:S(2)}, u32[]{:S(2)}) %all-to-all-start.2) | async-done | bytes 1048608 | tf_op jit(solution)/shard_map/all_to_all | solution.py:140
  278.0 3.3 %gather_fusion.2 = bf16[512,512]{1,0:T(8,128)(2,1)S(1)} fusion(bf16[1024,512]{1,0:T(8,128)(2,1)} %bitcast.25, s32[1024]{0:T(1024)S(1)} %pad_clamp_fusion), kind=kCustom, calls=%fused_computation.2 | custom fusion | bytes 1050624 | tf_op jit(solution)/shard_map/jit(_take)/gather | solution.py:143
  281.6 1.8 fusion.30
  283.4 3.4 %fusion.26 = bf16[256,512]{1,0:T(8,128)(2,1)} fusion(bf16[256,2048]{1,0:T(8,128)(2,1)} %all-gather.8.cloned.1.call-done, bf16[2048,512]{1,0:T(8,128)(2,1)} %param.27, f32[256,1,512]{2,1,0:T(1,128)} %fusion.30, bf16[256,512]{1,0:T(8,128)(2,1)S(1)} %copy-done.3), kind=kOutput, calls=%fused_computation.35 | convolution fusion | flops 537395200 | bytes 4194304 | tf_op jit(solution)/shard_map/dot_general | solution.py:138
  (82 shorter events, 7.2 us)
Async XLA Ops:
  6.5 234.7 %copy-start = (bf16[1,2048,512]{2,1,0:T(8,128)(2,1)S(1)}, bf16[1,2048,512]{2,1,0:T(8,128)(2,1)}, u32[]{:S(2)}) copy-start(bf16[1,2048,512]{2,1,0:T(8,128)(2,1)} %param.24) | copy-start | bytes 6291460
  7.8 5.5 %copy-start.2 = (bf16[2,256,256]{1,2,0:T(8,128)(2,1)}, bf16[2,256,256]{1,2,0:T(8,128)(2,1)S(1)}, u32[]{:S(2)}) copy-start(bf16[2,256,256]{1,2,0:T(8,128)(2,1)S(1)} %copy.63) | copy-start | bytes 786436
  7.8 10.9 %copy-start.4 = (bf16[256,256]{1,0:T(8,128)(2,1)S(1)}, bf16[256,256]{1,0:T(8,128)(2,1)}, u32[]{:S(2)}) copy-start(bf16[256,256]{1,0:T(8,128)(2,1)} %param.14) | copy-start | bytes 393220
  7.8 11.8 %collective-permute-start = (bf16[2,128,256]{1,2,0:T(8,128)(2,1)S(1)}, bf16[2,128,256]{1,2,0:T(8,128)(2,1)}, u32[]{:S(2)}, u32[]{:S(2)}) collective-permute-start(bf16[2,128,256]{1,2,0:T(8,128)(2,1)S(1)} %slice.34), channel_id=1, source_target_pairs={{0,4},{4,8},{8,12},{12,16},{16,20},{20,24},{24,28},{1,5},{5,9},{9,... | collective-permute-start | bytes 393224 | tf_op jit(solution)/shard_map/ppermute | solution.py:20
  13.3 29.4 %all-to-all-start = ((bf16[256,4,512]{0,2,1:T(8,128)(2,1)}), bf16[256,4,512]{0,2,1:T(8,128)(2,1)S(1)}, u32[]{:S(2)}, u32[]{:S(2)}) async-start(bf16[256,4,512]{0,2,1:T(8,128)(2,1)} %bitcast.91), calls=%async_computation | async-start | bytes 2097152 | tf_op jit(solution)/shard_map/all_to_all | solution.py:81
  17.8 54.0 %all-gather.6.cloned.1.call-start = ((), (), s32[]{:S(2)}) async-start(), calls=%async_computation.3 | async-start | bytes 1310720 | tf_op jit(solution)/shard_map/all_gather | solution.py:91
  22.0 5.6 %copy-start.6 = (pred[2,128,256]{1,2,0:T(8,128)(4,1)S(1)}, pred[2,128,256]{1,2,0:T(8,128)(4,1)}, u32[]{:S(2)}) copy-start(pred[2,128,256]{1,2,0:T(8,128)(4,1)} %broadcast_and_fusion) | copy-start | bytes 196612
  24.0 5.1 %copy-start.9 = (f32[4]{0:T(128)S(1)}, f32[4]{0:T(128)}, u32[]{:S(2)}) copy-start(f32[4]{0:T(128)} %param.16) | copy-start | bytes 52
  27.6 1.8 copy-start.5
  29.8 14.3 %copy-start.13 = (bf16[256,512]{1,0:T(8,128)(2,1)S(1)}, bf16[256,512]{1,0:T(8,128)(2,1)}, u32[]{:S(2)}) copy-start(bf16[256,512]{1,0:T(8,128)(2,1)} %param.18) | copy-start | bytes 786436
  42.7 4.0 %copy-start.7 = (s32[256,2]{0,1:T(2,128)S(1)}, s32[256,2]{0,1:T(2,128)}, u32[]{:S(2)}) copy-start(s32[256,2]{0,1:T(2,128)} %param.20) | copy-start | bytes 6148
  46.6 194.7 %all-gather.10.cloned.1.call-start = ((), (), s32[]{:S(2)}) async-start(), calls=%async_computation.5 | async-start | bytes 5242880 | tf_op jit(solution)/shard_map/all_gather | solution.py:133
  182.9 1.6 copy-start.10
  182.9 1.6 copy-start.14
  184.5 2.4 copy-start.11
  186.9 3.8 %copy-start.1 = (bf16[256,2048]{1,0:T(8,128)(2,1)S(1)}, bf16[256,2048]{1,0:T(8,128)(2,1)}, u32[]{:S(2)}) copy-start(bf16[256,2048]{1,0:T(8,128)(2,1)} %all-gather.6.cloned.1.call-done) | copy-start | bytes 3145732
  246.8 31.3 %all-to-all-start.2 = ((bf16[1,8,128,512]{3,2,0,1:T(8,128)(2,1)}), bf16[1,8,128,512]{3,2,0,1:T(8,128)(2,1)}, u32[]{:S(2)}, u32[]{:S(2)}) async-start(bf16[1,8,128,512]{3,2,0,1:T(8,128)(2,1)} %bitcast.93), calls=%async_computation.2 | async-start | bytes 2097152 | tf_op jit(solution)/shard_map/all_to_all | solution.py:140
  251.4 32.0 %all-gather.8.cloned.1.call-start = ((), (), s32[]{:S(2)}) async-start(), calls=%async_computation.4 | async-start | bytes 1310720 | tf_op jit(solution)/shard_map/all_gather | solution.py:134
  251.4 2.6 copy-start.12
  254.0 2.1 copy-start.8
  281.6 1.8 copy-start.3
Sparse Core Ops, SparseCore 0:
  46.7 25.0 all-gather.5
  190.8 50.3 all-gather.9
  255.8 26.7 all-gather.7
where the time goes:
time: 294 us; the launch traced here: 293 us
  blocking collectives  111 us (38%)
  waiting for transfers between devices  92.4 us (31%)
  local copies, waits for them, and re-layouts  30.1 us (10%)
  matrix products  25.3 us (9%)
  between operations  13.5 us (5%)
  starting transfers between devices  12.4 us (4%)
  other arithmetic  8.46 us (3%)
    all_to_all x1, blocking collectives, per_device(): lax.all_to_all(picked_rows.reshape(EXP_DEV, sp_count, capacity, stream_ro...  98.4 us
    all_gather x1, waiting for transfers between devices, per_device(): routed_piece = lax.all_gather(hidden, 'tp', axis=2, tiled=True)  50.3 us
    all_to_all x1, waiting for transfers between devices, per_device(): lax.all_to_all(outgoing, 'sp', split_axis=1, concat_axis=1, tiled=True)  21.8 us
    all_gather x1, waiting for transfers between devices, per_device(): stream_rows = lax.all_gather(stream_cols, 'tp', axis=1, tiled=True)  20.4 us
    all_gather x1, blocking collectives, per_device(): attended_all = lax.all_gather(attended_values, 'tp', axis=1, tiled=True)  12.7 us
    gather x1, local copies, waits for them, and re-layouts, per_device(): jnp.take(stream_rows, slot_owner, axis=0, mode='fill', fill_value=0)  10.2 us
  transfers between devices with their start and end apart: 6, of which 3 were waited for; matrix products, arithmetic and copies ran while one was open for 10% of the time, Pallas kernels for 0%

commit v1 on v0

--- a/solution.py
+++ b/solution.py
@@ -88,7 +88,12 @@
     column_share = column_share.reshape(HEADS * HEAD_WIDTH, col_width)
     feature_sum = jnp.dot(attended_all, column_share, preferred_element_type=jnp.float32)
     stream_cols = (feature_sum + residual.astype(jnp.float32)).astype(jnp.bfloat16)
-    stream_rows = lax.all_gather(stream_cols, "tp", axis=1, tiled=True)
+    ring = [stream_cols]
+    for hop in range(3):
+        ring.append(lax.ppermute(ring[-1], "tp", [(dev, (dev + 1) % 4) for dev in range(4)]))
+    stream_rows = jnp.roll(
+        jnp.concatenate(ring[::-1], axis=1), (lax.axis_index("tp") + 1) * ring[0].shape[1], axis=1
+    )
     gate_eff = (norm_gain[None, :, None] * gate_weight.astype(jnp.float32)).astype(jnp.bfloat16)
     up_eff = (norm_gain[None, :, None] * up_weight.astype(jnp.float32)).astype(jnp.bfloat16)
     shared_gate_eff = (norm_gain[:, None] * shared_gate.astype(jnp.float32)).astype(jnp.bfloat16)

time: 294 us -> 294 us (level)
    all_gather x1 -> x0, waiting for transfers between devices: 20.4 us -> none  [per_device(): stream_rows = lax.all_gather(stream_cols, 'tp', axis=1, tiled=True)]
    ppermute x0 -> x3, waiting for transfers between devices: none -> 20 us  [per_device(): lax.ppermute(ring[-1], 'tp', [(dev, (dev + 1) % 4) for dev in range(4)])]
    gather x1, local copies, waits for them, and re-layouts: 10.2 us -> 6 us  [per_device(): jnp.take(stream_rows, slot_owner, axis=0, mode='fill', fill_value=0)]
  transfers between devices with their start and end apart: 6 -> 8, of which waited for: 3 -> 5; matrix products, arithmetic and copies ran while one was open for 10% -> 11% of each run, Pallas kernels for 0% -> 0%
where the time goes in v1:
time: 294 us; the launch traced here: 293 us
  blocking collectives  110 us (37%)
  waiting for transfers between devices  93.7 us (32%)
  local copies, waits for them, and re-layouts  28.1 us (10%)
  matrix products  24.5 us (8%)
  between operations  13.8 us (5%)
  starting transfers between devices  13.3 us (5%)
  other arithmetic  9.64 us (3%)
    all_to_all x1, blocking collectives, per_device(): lax.all_to_all(picked_rows.reshape(EXP_DEV, sp_count, capacity, stream_ro...  96.9 us
    all_gather x1, waiting for transfers between devices, per_device(): routed_piece = lax.all_gather(hidden, 'tp', axis=2, tiled=True)  52.5 us
    all_to_all x1, waiting for transfers between devices, per_device(): lax.all_to_all(outgoing, 'sp', split_axis=1, concat_axis=1, tiled=True)  21.2 us
    ppermute x3, waiting for transfers between devices, per_device(): lax.ppermute(ring[-1], 'tp', [(dev, (dev + 1) % 4) for dev in range(4)])  20 us
    all_gather x1, blocking collectives, per_device(): attended_all = lax.all_gather(attended_values, 'tp', axis=1, tiled=True)  12.8 us
    gather x1, local copies, waits for them, and re-layouts, per_device(): jnp.take(stream_rows, slot_owner, axis=0, mode='fill', fill_value=0)  6 us
  transfers between devices with their start and end apart: 8, of which 5 were waited for; matrix products, arithmetic and copies ran while one was open for 11% of the time, Pallas kernels for 0%

profile of v1, /device:TPU:0, one launch (start us, length us, event | category | flops | bytes accessed | tf_op | source)
XLA Modules:
  0.0 292.8 jit_solution(9569816941855985741)
XLA Ops:
  6.5 1.2 copy.63
  8.5 3.2 %collective-permute-start = (bf16[2,128,256]{1,2,0:T(8,128)(2,1)}, bf16[2,128,256]{1,2,0:T(8,128)(2,1)}, u32[]{:S(2)}, u32[]{:S(2)}) collective-permute-start(bf16[2,128,256]{1,2,0:T(8,128)(2,1)} %slice.34), channel_id=1, source_target_pairs={{0,4},{4,8},{8,12},{12,16},{16,20},{20,24},{24,28},{1,5},{5,9},{9,... | collective-permute-start | bytes 393224 | tf_op jit(solution)/shard_map/ppermute | solution.py:20
  11.7 2.3 copy.73
  13.9 4.5 %all-to-all-start = ((bf16[256,4,512]{0,2,1:T(8,128)(2,1)}), bf16[256,4,512]{0,2,1:T(8,128)(2,1)S(1)}, u32[]{:S(2)}, u32[]{:S(2)}) async-start(bf16[256,4,512]{0,2,1:T(8,128)(2,1)} %bitcast.91), calls=%async_computation | async-start | bytes 2097152 | tf_op jit(solution)/shard_map/all_to_all | solution.py:81
  18.9 1.1 reduce-window.6
  23.9 1.0 pad_maximum_fusion
  24.9 1.5 gather_fusion
  26.4 1.1 select_bitcast_fusion
  28.5 1.0 reshape.382
  30.3 1.0 reshape.383
  32.1 1.5 fusion.48
  34.4 12.8 %all_gather.9 = bf16[256,1024]{0,1:T(8,128)(2,1)} all-gather(bf16[256,256]{0,1:T(8,128)(2,1)S(1)} %bitcast.95), channel_id=1, replica_groups=mesh['sp'=8,'tp'=4] {'tp'}, dimensions={1}, use_global_device_ids=true | all-gather | bytes 655360 | tf_op jit(solution)/shard_map/all_gather | solution.py:79
  47.2 1.3 copy.74
  48.5 1.9 fusion.25
  51.4 7.7 %collective-permute-done.1 = bf16[256,512]{1,0:T(8,128)(2,1)S(1)} collective-permute-done((bf16[256,512]{1,0:T(8,128)(2,1)S(1)}, bf16[256,512]{1,0:T(8,128)(2,1)S(1)}, u32[]{:S(2)}, u32[]{:S(2)}) %collective-permute-start.1) | collective-permute-done | bytes 262176 | tf_op jit(solution)/shard_map/ppermute | solution.py:93
  59.4 2.4 scatter_custom_fusion
  61.9 5.0 %collective-permute-done.2 = bf16[256,512]{1,0:T(8,128)(2,1)S(1)} collective-permute-done((bf16[256,512]{1,0:T(8,128)(2,1)S(1)}, bf16[256,512]{1,0:T(8,128)(2,1)S(1)}, u32[]{:S(2)}, u32[]{:S(2)}) %collective-permute-start.2) | collective-permute-done | bytes 262176 | tf_op jit(solution)/shard_map/ppermute | solution.py:93
  67.0 7.2 %collective-permute-done.3 = bf16[256,512]{1,0:T(8,128)(2,1)S(1)} collective-permute-done((bf16[256,512]{1,0:T(8,128)(2,1)S(1)}, bf16[256,512]{1,0:T(8,128)(2,1)S(1)}, u32[]{:S(2)}, u32[]{:S(2)}) %collective-permute-start.3) | collective-permute-done | bytes 262176 | tf_op jit(solution)/shard_map/ppermute | solution.py:93
  74.7 6.0 %gather_fusion.1 = bf16[1024,2048]{1,0:T(8,128)(2,1)} fusion(bf16[256,2048]{1,0:T(8,128)(2,1)S(1)} %get-tuple-element.6, s32[1024]{0:T(1024)S(1)} %fusion.39), kind=kCustom, calls=%fused_computation.1 | custom fusion | bytes 8392704 | tf_op jit(solution)/shard_map/jit(_take)/gather | solution.py:117
  80.7 2.5 broadcast_select_fusion
  83.3 96.9 %all_to_all.25 = bf16[1,8,128,2048]{3,2,0,1:T(8,128)(2,1)S(1)} all-to-all(bf16[1,8,128,2048]{3,2,0,1:T(8,128)(2,1)S(1)} %broadcast_select_fusion), channel_id=1, replica_groups=mesh['sp'=8,'tp'=4] {'sp'}, dimensions={1} | all-to-all | bytes 8388608 | tf_op jit(solution)/shard_map/all_to_all | solution.py:118
  181.8 2.4 fusion.3
  184.2 3.7 %multiply_convert_fusion.6 = bf16[1024,512]{1,0:T(8,128)(2,1)} fusion(f32[1024,512]{1,0:T(8,128)S(1)} %fusion.3, bf16[1024,2048]{1,0:T(8,128)(2,1)S(1)} %bitcast.89, bf16[1,2048,512]{2,1,0:T(8,128)(2,1)S(1)} %copy-done.12, f32[2048]{0:T(1024)S(1)} %copy-done.14, f32[1024]{0:T(1024)S(1)} %rsqrt_bitcast_fusion), kind=kOutput, calls=%fused_computation.18 | convolution fusion | flops 2154823680 | bytes 9449472 | tf_op jit(solution)/shard_map/erd,edf->erf/dot_general | solution.py:128
  188.0 52.5 %all-gather.7.cloned.1.call-done = bf16[1024,2048]{1,0:T(8,128)(2,1)} async-done(((bf16[1024,512]{1,0:T(8,128)(2,1)}), bf16[1024,2048]{1,0:T(8,128)(2,1)}) %all-gather.7.cloned.1.call-update) | async-done | bytes 4194320 | tf_op jit(solution)/shard_map/all_gather | solution.py:138
  240.5 5.5 %fusion.16 = bf16[1024,512]{1,0:T(8,128)(2,1)} fusion(bf16[1024,2048]{1,0:T(8,128)(2,1)} %all-gather.7.cloned.1.call-done, bf16[1,2048,512]{2,1,0:T(8,128)(2,1)S(1)} %copy-done), kind=kOutput, calls=%fused_computation.24 | convolution fusion | flops 2148007936 | bytes 7340032 | tf_op jit(solution)/shard_map/erf,efd->erd/dot_general | solution.py:140
  246.0 4.6 %all-to-all-start.2 = ((bf16[1,8,128,512]{3,2,0,1:T(8,128)(2,1)}), bf16[1,8,128,512]{3,2,0,1:T(8,128)(2,1)}, u32[]{:S(2)}, u32[]{:S(2)}) async-start(bf16[1,8,128,512]{3,2,0,1:T(8,128)(2,1)} %bitcast.93), calls=%async_computation.2 | async-start | bytes 2097152 | tf_op jit(solution)/shard_map/all_to_all | solution.py:145
  250.6 2.6 fusion.23
  253.2 1.6 fusion.27
  256.1 21.2 %all-to-all-done.2 = bf16[1,8,128,512]{3,2,0,1:T(8,128)(2,1)} async-done(((bf16[1,8,128,512]{3,2,0,1:T(8,128)(2,1)}), bf16[1,8,128,512]{3,2,0,1:T(8,128)(2,1)}, u32[]{:S(2)}, u32[]{:S(2)}) %all-to-all-start.2) | async-done | bytes 1048608 | tf_op jit(solution)/shard_map/all_to_all | solution.py:145
  277.3 3.3 %gather_fusion.2 = bf16[512,512]{1,0:T(8,128)(2,1)S(1)} fusion(bf16[1024,512]{1,0:T(8,128)(2,1)} %bitcast.25, s32[1024]{0:T(1024)S(1)} %pad_clamp_fusion), kind=kCustom, calls=%fused_computation.2 | custom fusion | bytes 1050624 | tf_op jit(solution)/shard_map/jit(_take)/gather | solution.py:148
  280.8 1.8 fusion.30
  282.6 3.3 %fusion.26 = bf16[256,512]{1,0:T(8,128)(2,1)} fusion(bf16[256,2048]{1,0:T(8,128)(2,1)} %all-gather.5.cloned.1.call-done, bf16[2048,512]{1,0:T(8,128)(2,1)} %param.27, f32[256,1,512]{2,1,0:T(1,128)S(1)} %fusion.30, bf16[256,512]{1,0:T(8,128)(2,1)S(1)} %fusion.25), kind=kOutput, calls=%fused_computation.35 | convolution fusion | flops 537395200 | bytes 4194304 | tf_op jit(solution)/shard_map/dot_general | solution.py:143
  (94 shorter events, 13.1 us)
Async XLA Ops:
  6.5 234.0 %copy-start = (bf16[1,2048,512]{2,1,0:T(8,128)(2,1)S(1)}, bf16[1,2048,512]{2,1,0:T(8,128)(2,1)}, u32[]{:S(2)}) copy-start(bf16[1,2048,512]{2,1,0:T(8,128)(2,1)} %param.24) | copy-start | bytes 6291460
  7.8 6.2 %copy-start.1 = (bf16[2,256,256]{1,2,0:T(8,128)(2,1)}, bf16[2,256,256]{1,2,0:T(8,128)(2,1)S(1)}, u32[]{:S(2)}) copy-start(bf16[2,256,256]{1,2,0:T(8,128)(2,1)S(1)} %copy.63) | copy-start | bytes 786436
  8.5 10.2 %copy-start.5 = (s32[256,2]{0,1:T(2,128)S(1)}, s32[256,2]{0,1:T(2,128)}, u32[]{:S(2)}) copy-start(s32[256,2]{0,1:T(2,128)} %param.20) | copy-start | bytes 6148
  8.5 13.9 %copy-start.2 = (bf16[256,256]{1,0:T(8,128)(2,1)S(1)}, bf16[256,256]{1,0:T(8,128)(2,1)}, u32[]{:S(2)}) copy-start(bf16[256,256]{1,0:T(8,128)(2,1)} %param.14) | copy-start | bytes 393220
  8.5 15.4 %collective-permute-start = (bf16[2,128,256]{1,2,0:T(8,128)(2,1)}, bf16[2,128,256]{1,2,0:T(8,128)(2,1)}, u32[]{:S(2)}, u32[]{:S(2)}) collective-permute-start(bf16[2,128,256]{1,2,0:T(8,128)(2,1)} %slice.34), channel_id=1, source_target_pairs={{0,4},{4,8},{8,12},{12,16},{16,20},{20,24},{24,28},{1,5},{5,9},{9,... | collective-permute-start | bytes 393224 | tf_op jit(solution)/shard_map/ppermute | solution.py:20
  13.9 33.2 %all-to-all-start = ((bf16[256,4,512]{0,2,1:T(8,128)(2,1)}), bf16[256,4,512]{0,2,1:T(8,128)(2,1)S(1)}, u32[]{:S(2)}, u32[]{:S(2)}) async-start(bf16[256,4,512]{0,2,1:T(8,128)(2,1)} %bitcast.91), calls=%async_computation | async-start | bytes 2097152 | tf_op jit(solution)/shard_map/all_to_all | solution.py:81
  18.5 222.0 %all-gather.7.cloned.1.call-start = ((), (), s32[]{:S(2)}) async-start(), calls=%async_computation.4 | async-start | bytes 5242880 | tf_op jit(solution)/shard_map/all_gather | solution.py:138
  23.3 0.6 copy-start.7
  26.4 5.7 %copy-start.4 = (pred[2,128,256]{1,2,0:T(8,128)(4,1)S(1)}, pred[2,128,256]{1,2,0:T(8,128)(4,1)}, u32[]{:S(2)}) copy-start(pred[2,128,256]{1,2,0:T(8,128)(4,1)} %broadcast_and_fusion) | copy-start | bytes 196612
  28.5 5.1 %copy-start.10 = (f32[4]{0:T(128)S(1)}, f32[4]{0:T(128)}, u32[]{:S(2)}) copy-start(f32[4]{0:T(128)} %param.16) | copy-start | bytes 52
  32.1 1.8 copy-start.3
  47.2 4.1 %slice-start = ((s32[8,5]{0,1:T(8,128)}), s32[8,4]{0,1:T(4,128)S(1)}, s32[]{:S(2)}) async-start(s32[8,5]{0,1:T(8,128)} %copy-done.7), calls=%async_computation.5 | async-start | bytes 4096 | tf_op jit(solution)/shard_map/slice.1
  47.2 4.1 %copy-start.8 = (s32[512]{0:T(512)S(1)}, s32[512]{0:T(512)}, u32[]{:S(2)}) copy-start(s32[512]{0:T(512)} %reshape.334) | copy-start | bytes 6148
  47.2 4.2 %copy-start.6 = (s32[256,2]{0,1:T(2,128)S(1)}, s32[256,2]{0,1:T(2,128)}, u32[]{:S(2)}) copy-start(s32[256,2]{0,1:T(2,128)} %param.20) | copy-start | bytes 6148
  50.4 8.7 %collective-permute-start.1 = (bf16[256,512]{1,0:T(8,128)(2,1)S(1)}, bf16[256,512]{1,0:T(8,128)(2,1)S(1)}, u32[]{:S(2)}, u32[]{:S(2)}) collective-permute-start(bf16[256,512]{1,0:T(8,128)(2,1)S(1)} %fusion.25), channel_id=1, source_target_pairs={{0,1},{1,2},{2,3},{3,0},{4,5},{5,6},{6,7},{7,4},{8,9},{9,10},{10,1... | collective-permute-start | bytes 786440 | tf_op jit(solution)/shard_map/ppermute | solution.py:93
  59.1 7.8 %collective-permute-start.2 = (bf16[256,512]{1,0:T(8,128)(2,1)S(1)}, bf16[256,512]{1,0:T(8,128)(2,1)S(1)}, u32[]{:S(2)}, u32[]{:S(2)}) collective-permute-start(bf16[256,512]{1,0:T(8,128)(2,1)S(1)} %collective-permute-done.1), channel_id=1, source_target_pairs={{0,1},{1,2},{2,3},{3,0},{4,5},{5,6},{6,7},{7,4},{8,9},{9,10},{10,1... | collective-permute-start | bytes 786440 | tf_op jit(solution)/shard_map/ppermute | solution.py:93
  66.9 7.3 %collective-permute-start.3 = (bf16[256,512]{1,0:T(8,128)(2,1)S(1)}, bf16[256,512]{1,0:T(8,128)(2,1)S(1)}, u32[]{:S(2)}, u32[]{:S(2)}) collective-permute-start(bf16[256,512]{1,0:T(8,128)(2,1)S(1)} %collective-permute-done.2), channel_id=1, source_target_pairs={{0,1},{1,2},{2,3},{3,0},{4,5},{5,6},{6,7},{7,4},{8,9},{9,10},{10,1... | collective-permute-start | bytes 786440 | tf_op jit(solution)/shard_map/ppermute | solution.py:93
  180.2 1.6 copy-start.11
  180.2 1.6 copy-start.14
  181.8 2.4 copy-start.12
  246.0 31.3 %all-to-all-start.2 = ((bf16[1,8,128,512]{3,2,0,1:T(8,128)(2,1)}), bf16[1,8,128,512]{3,2,0,1:T(8,128)(2,1)}, u32[]{:S(2)}, u32[]{:S(2)}) async-start(bf16[1,8,128,512]{3,2,0,1:T(8,128)(2,1)} %bitcast.93), calls=%async_computation.2 | async-start | bytes 2097152 | tf_op jit(solution)/shard_map/all_to_all | solution.py:145
  250.6 32.0 %all-gather.5.cloned.1.call-start = ((), (), s32[]{:S(2)}) async-start(), calls=%async_computation.3 | async-start | bytes 1310720 | tf_op jit(solution)/shard_map/all_gather | solution.py:139
  250.6 2.6 copy-start.13
  253.2 2.6 copy-start.9
Sparse Core Ops, SparseCore 0:
  188.1 52.3 all-gather.6
  255.0 26.8 all-gather.4
